TPU v7x, 32 devices: a whole 2x2x4 slice. The times are simulated.
32 devices in a mesh: grp: 2 (over y), fs: 4 (over z), tp: 4 (over x, core).
Axes of the slice: x: 2, y: 2, z: 4, core: 2. Of those that a mesh axis runs over, the one named last changes fastest.
Arguments:
- tokens: bfloat16 [4096, 2048], P(('grp', 'fs'), 'tp'), parts along dimension 0, may hold values from -6 to 6
- first_gain: bfloat16 [2048], replicated, may hold values from 0.099609375 to 1.8984375
- u_proj: bfloat16 [2048, 1024], P('fs', 'tp'), may hold values from -0.125 to 0.125
- v_proj: bfloat16 [2048, 1024], P('fs', 'tp'), may hold values from -0.125 to 0.125
- group_gain: bfloat16 [8, 128], P('tp'), may hold values from 0.099609375 to 1.8984375
- spatial: bfloat16 [8, 128, 128], P('tp'), may hold values from -0.5 to 0.5
- spatial_bias: bfloat16 [8, 128], P('tp'), may hold values from 0.099609375 to 1.8984375
- mix_proj: bfloat16 [1024, 2048], P('fs', 'tp'), may hold values from -0.1875 to 0.1875
- second_gain: bfloat16 [2048], replicated, may hold values from 0.099609375 to 1.8984375
- up_proj: bfloat16 [2048, 8192], P('fs', 'tp'), may hold values from -0.125 to 0.125
- down_proj: bfloat16 [8192, 2048], P('tp', 'fs'), may hold values from -0.0625 to 0.0625
Outputs:
- layer_out: bfloat16 [4096, 2048], P(('grp', 'fs'), 'tp'), parts along dimension 0
There are 2 independent parts, one for each index of `grp`. A program takes and returns all parts, laid end to end along the dimension named above; an argument that names none is the same for every part. Nothing has to cross between parts.
All inputs are finite; a program needn't handle non-finite values.
Results may differ from a plain program's by a relative error of at most 0.017.
Values may be sent and summed in bfloat16 or wider, within the bound.
A program may use at most 64 MiB of HBM per device.

v0:
```python
import jax
import jax.numpy as jnp
from jax import lax
from jax.sharding import PartitionSpec as P

EPS = 1e-06


def rms_scale(values, gain_vec):
    mean_sq = jnp.mean(values * values, axis=-1, keepdims=True)
    return values * lax.rsqrt(mean_sq + EPS) * gain_vec.astype(jnp.float32)


def per_device(
    tokens,
    first_gain,
    u_proj,
    v_proj,
    group_gain,
    spatial,
    spatial_bias,
    mix_proj,
    second_gain,
    up_proj,
    down_proj,
):
    whole_rows = lax.all_gather(tokens, "tp", axis=1, tiled=True)
    row_count = whole_rows.shape[0]
    normed_rows = rms_scale(whole_rows.astype(jnp.float32), first_gain).astype(jnp.bfloat16)
    local_width = u_proj.shape[1]
    column_part = normed_rows
    u_pre = jnp.dot(
        column_part,
        lax.all_gather(u_proj, "fs", axis=0, tiled=True),
        preferred_element_type=jnp.float32,
    )
    v_pre = jnp.dot(
        column_part,
        lax.all_gather(v_proj, "fs", axis=0, tiled=True),
        preferred_element_type=jnp.float32,
    )
    u_act = jax.nn.gelu(u_pre).astype(jnp.bfloat16)
    local_groups = group_gain.shape[0]
    group_width = group_gain.shape[1]
    v_groups = jax.nn.gelu(v_pre).reshape(row_count, local_groups, group_width)
    v_normed = rms_scale(v_groups, group_gain).astype(jnp.bfloat16)
    block_len = spatial.shape[1]
    block_view = v_normed.reshape(row_count // block_len, block_len, local_groups, group_width)
    causal_mask = jnp.tril(jnp.ones((block_len, block_len), jnp.bool_))
    masked_weights = jnp.where(causal_mask[None], spatial, jnp.zeros_like(spatial))
    mixed_vals = jnp.einsum(
        "gts,nsgd->ntgd", masked_weights, block_view, preferred_element_type=jnp.float32
    )
    mixed_vals = mixed_vals + spatial_bias.astype(jnp.float32).T[None, :, :, None]
    gated_vals = (u_act.astype(jnp.float32) * mixed_vals.reshape(row_count, local_width)).astype(
        jnp.bfloat16
    )
    gated_whole = lax.all_gather(gated_vals, "tp", axis=1, tiled=True)
    column_part = gated_whole
    mix_vals = jnp.dot(
        column_part,
        lax.all_gather(mix_proj, "fs", axis=0, tiled=True),
        preferred_element_type=jnp.float32,
    )
    mid_stream = (tokens.astype(jnp.float32) + mix_vals).astype(jnp.bfloat16)
    mid_whole = lax.all_gather(mid_stream, "tp", axis=1, tiled=True)
    normed_two = rms_scale(mid_whole.astype(jnp.float32), second_gain).astype(jnp.bfloat16)
    column_part = normed_two
    pre_act = jnp.dot(
        column_part,
        lax.all_gather(up_proj, "fs", axis=0, tiled=True),
        preferred_element_type=jnp.float32,
    )
    hidden_act = jnp.square(jax.nn.relu(pre_act)).astype(jnp.bfloat16)
    down_terms = jnp.dot(
        hidden_act,
        lax.all_gather(down_proj, "fs", axis=1, tiled=True),
        preferred_element_type=jnp.float32,
    )
    down_sum = lax.psum_scatter(
        down_terms.astype(jnp.bfloat16), "tp", scatter_dimension=1, tiled=True
    ).astype(jnp.float32)
    return (mid_stream.astype(jnp.float32) + down_sum).astype(jnp.bfloat16)


def solution(mesh):
    return jax.shard_map(
        per_device,
        mesh=mesh,
        in_specs=(
            P(("grp", "fs"), "tp"),
            P(),
            P("fs", "tp"),
            P("fs", "tp"),
            P("tp", None),
            P("tp", None, None),
            P("tp", None),
            P("fs", "tp"),
            P(),
            P("fs", "tp"),
            P("tp", "fs"),
        ),
        out_specs=P(("grp", "fs"), "tp"),
        check_vma=False,
    )
```

profile of v0, /device:TPU:0, one launch (start us, length us, event | category | flops | bytes accessed | tf_op | source)
XLA Modules:
  0.0 520.2 jit_solution(6290348988835134259)
XLA Ops:
  6.5 0.7 all-gather.9.cloned.1.call-update
  7.3 0.7 all-gather.13.cloned.1.call-update
  8.1 0.7 all-gather.11.cloned.1.call-update
  9.4 0.7 convert_element_type.58
  11.4 22.8 %all-gather.9.cloned.1.call-done = bf16[512,2048]{1,0:T(8,128)(2,1)} async-done(((bf16[512,512]{1,0:T(8,128)(2,1)}), bf16[512,2048]{1,0:T(8,128)(2,1)}) %all-gather.9.cloned.1.call-update) | async-done | bytes 2097168 | tf_op jit(solution)/shard_map/all_gather | solution.py:27
  34.2 2.1 fusion
  36.3 27.5 %all-gather.13.cloned.1.call-done = bf16[2048,256]{1,0:T(8,128)(2,1)} async-done(((bf16[512,256]{1,0:T(8,128)(2,1)}), bf16[2048,256]{1,0:T(8,128)(2,1)}) %all-gather.13.cloned.1.call-update) | async-done | bytes 1048592 | tf_op jit(solution)/shard_map/all_gather | solution.py:39
  63.8 3.5 fusion.52
  68.3 1.3 reshape.52
  70.2 1.0 copy.26
  71.2 21.6 %all-gather.11.cloned.1.call-done = bf16[2048,256]{1,0:T(8,128)(2,1)} async-done(((bf16[512,256]{1,0:T(8,128)(2,1)}), bf16[2048,256]{1,0:T(8,128)(2,1)}) %all-gather.11.cloned.1.call-update) | async-done | bytes 1048592 | tf_op jit(solution)/shard_map/all_gather | solution.py:34
  92.8 2.9 fusion.33
  95.8 25.8 %all-gather.17.cloned.1.call-done = bf16[1024,512]{1,0:T(8,128)(2,1)} async-done(((bf16[256,512]{1,0:T(8,128)(2,1)}), bf16[1024,512]{1,0:T(8,128)(2,1)}) %all-gather.17.cloned.1.call-update) | async-done | bytes 1048592 | tf_op jit(solution)/shard_map/all_gather | solution.py:62
  121.6 17.6 %all-gather.15.cloned.1.call-done = bf16[512,1024]{1,0:T(8,128)(2,1)} async-done(((bf16[512,256]{1,0:T(8,128)(2,1)}), bf16[512,1024]{1,0:T(8,128)(2,1)}) %all-gather.15.cloned.1.call-update) | async-done | bytes 1048592 | tf_op jit(solution)/shard_map/all_gather | solution.py:58
  139.2 3.0 fusion.9
  142.3 0.7 all-gather.21.cloned.1.call-update
  143.1 0.7 all-gather.23.cloned.1.call-update
  143.9 21.1 %all-gather.19.cloned.1.call-done = bf16[512,2048]{1,0:T(8,128)(2,1)} async-done(((bf16[512,512]{1,0:T(8,128)(2,1)}), bf16[512,2048]{1,0:T(8,128)(2,1)}) %all-gather.19.cloned.1.call-update) | async-done | bytes 2097168 | tf_op jit(solution)/shard_map/all_gather | solution.py:66
  165.0 2.1 fusion.3
  167.1 149.1 %all-gather.21.cloned.1.call-done = bf16[2048,2048]{1,0:T(8,128)(2,1)} async-done(((bf16[512,2048]{1,0:T(8,128)(2,1)}), bf16[2048,2048]{1,0:T(8,128)(2,1)}) %all-gather.21.cloned.1.call-update) | async-done | bytes 8388624 | tf_op jit(solution)/shard_map/all_gather | solution.py:71
  316.2 149.4 %all-gather.23.cloned.1.call-done = bf16[2048,2048]{1,0:T(8,128)(2,1)} async-done(((bf16[2048,512]{1,0:T(8,128)(2,1)}), bf16[2048,2048]{1,0:T(8,128)(2,1)}) %all-gather.23.cloned.1.call-update) | async-done | bytes 8388624 | tf_op jit(solution)/shard_map/all_gather | solution.py:77
  465.6 16.6 %convolution_convert_fusion = bf16[512,2048]{1,0:T(8,128)(2,1)} fusion(bf16[2048,2048]{1,0:T(8,128)(2,1)} %all-gather.23.cloned.1.call-done, bf16[2048,2048]{1,0:T(8,128)(2,1)} %all-gather.21.cloned.1.call-done, bf16[512,2048]{1,0:T(8,128)(2,1)} %all-gather.19.cloned.1.call-done, f32[2048]{0:T(1024)S(1)} %convert_element_type.68, f32[512]{0:T(512)S(1)} %add_rsqrt_fusion.1), kind=kOutput, calls=%fused_computation.11 | convolution fusion | flops 8598323200 | bytes 20981760 | tf_op jit(solution)/shard_map/dot_general | solution.py:75
  482.2 29.5 %reduce-scatter.2.cloned.1.call-done = bf16[512,512]{1,0:T(8,128)(2,1)} async-done(((bf16[512,2048]{1,0:T(8,128)(2,1)}), bf16[512,512]{1,0:T(8,128)(2,1)}) %reduce-scatter.2.cloned.1.call-update) | async-done | bytes 524304 | tf_op jit(solution)/shard_map/reduce_scatter | solution.py:80
  511.7 2.0 add_convert_fusion
  (35 shorter events, 3.8 us)
Async XLA Ops:
  6.5 27.7 %all-gather.9.cloned.1.call-start = ((), (), s32[]{:S(2)}) async-start(), calls=%async_computation.1 | async-start | bytes 2621440 | tf_op jit(solution)/shard_map/all_gather | solution.py:27
  7.3 56.5 %all-gather.13.cloned.1.call-start = ((), (), s32[]{:S(2)}) async-start(), calls=%async_computation.3 | async-start | bytes 1310720 | tf_op jit(solution)/shard_map/all_gather | solution.py:39
  8.0 84.8 %all-gather.11.cloned.1.call-start = ((), (), s32[]{:S(2)}) async-start(), calls=%async_computation.2 | async-start | bytes 1310720 | tf_op jit(solution)/shard_map/all_gather | solution.py:34
  8.7 112.9 %all-gather.17.cloned.1.call-start = ((), (), s32[]{:S(2)}) async-start(), calls=%async_computation.5 | async-start | bytes 1310720 | tf_op jit(solution)/shard_map/all_gather | solution.py:62
  9.3 129.9 %all-gather.15.cloned.1.call-start = ((), (), s32[]{:S(2)}) async-start(), calls=%async_computation.4 | async-start | bytes 1310720 | tf_op jit(solution)/shard_map/all_gather | solution.py:58
  36.3 33.6 %copy-start.3 = (bf16[2,128,128]{2,1,0:T(8,128)(2,1)S(1)}, bf16[2,128,128]{2,1,0:T(8,128)(2,1)}, u32[]{:S(2)}) copy-start(bf16[2,128,128]{2,1,0:T(8,128)(2,1)} %param.16) | copy-start | bytes 196612
  67.3 25.5 %copy-start.1 = (bf16[512,2048]{1,0:T(8,128)(2,1)S(1)}, bf16[512,2048]{1,0:T(8,128)(2,1)}, u32[]{:S(2)}) copy-start(bf16[512,2048]{1,0:T(8,128)(2,1)} %all-gather.9.cloned.1.call-done) | copy-start | bytes 6291460
  70.2 69.1 %copy-start.2 = (bf16[512,512]{1,0:T(8,128)(2,1)S(1)}, bf16[512,512]{1,0:T(8,128)(2,1)}, u32[]{:S(2)}) copy-start(bf16[512,512]{1,0:T(8,128)(2,1)} %param.11) | copy-start | bytes 1572868
  95.7 48.1 %copy-start.4 = (bf16[2048]{0:T(1024)(128)(2,1)S(1)}, bf16[2048]{0:T(1024)(128)(2,1)}, u32[]{:S(2)}) copy-start(bf16[2048]{0:T(1024)(128)(2,1)} %param.19) | copy-start | bytes 12292
  95.7 69.3 %all-gather.19.cloned.1.call-start = ((), (), s32[]{:S(2)}) async-start(), calls=%async_computation.6 | async-start | bytes 2621440 | tf_op jit(solution)/shard_map/all_gather | solution.py:66
  142.3 173.9 %all-gather.21.cloned.1.call-start = ((), (), s32[]{:S(2)}) async-start(), calls=%async_computation.7 | async-start | bytes 10485760 | tf_op jit(solution)/shard_map/all_gather | solution.py:71
  143.0 322.6 %all-gather.23.cloned.1.call-start = ((), (), s32[]{:S(2)}) async-start(), calls=%async_computation.8 | async-start | bytes 10485760 | tf_op jit(solution)/shard_map/all_gather | solution.py:77
  143.8 367.9 %reduce-scatter.2.cloned.1.call-start = ((), (), s32[]{:S(2)}) async-start(), calls=%async_computation.9 | async-start | bytes 2621440 | tf_op jit(solution)/shard_map/reduce_scatter | solution.py:80
  167.1 344.6 %copy-start = (bf16[512,512]{1,0:T(8,128)(2,1)S(1)}, bf16[512,512]{1,0:T(8,128)(2,1)}, u32[]{:S(2)}) copy-start(bf16[512,512]{1,0:T(8,128)(2,1)} %fusion.9) | copy-start | bytes 1572868
Sparse Core Ops, SparseCore 0:
  8.9 25.2 all-gather.8
  35.8 27.9 all-gather.12
  65.4 27.3 all-gather.10
  94.2 27.3 all-gather.16
  123.0 16.1 all-gather.14
  142.4 22.5 all-gather.18
  166.6 149.6 all-gather.20
  317.8 147.7 all-gather.22
  482.3 29.3 reduce-scatter.1
where the time goes:
time: 521 us; the launch traced here: 520 us
  waiting for transfers between devices  469 us (90%)
  matrix products  26.3 us (5%)
  between operations  13.3 us (3%)
  other arithmetic  8.82 us (2%)
    all_gather x1, waiting for transfers between devices, per_device(): lax.all_gather(down_proj, 'fs', axis=1, tiled=True)  149 us
    all_gather x1, waiting for transfers between devices, per_device(): lax.all_gather(up_proj, 'fs', axis=0, tiled=True)  149 us
    reduce_scatter x1, waiting for transfers between devices, per_device(): lax.psum_scatter(down_terms.astype(jnp.bfloat16), 'tp', scatter_dimension...  29.5 us
    all_gather x1, waiting for transfers between devices, per_device(): lax.all_gather(v_proj, 'fs', axis=0, tiled=True)  27.5 us
    all_gather x1, waiting for transfers between devices, per_device(): lax.all_gather(mix_proj, 'fs', axis=0, tiled=True)  25.8 us
    all_gather x1, waiting for transfers between devices, per_device(): whole_rows = lax.all_gather(tokens, 'tp', axis=1, tiled=True)  22.8 us
    all_gather x1, waiting for transfers between devices, per_device(): lax.all_gather(u_proj, 'fs', axis=0, tiled=True)  21.6 us
    all_gather x1, waiting for transfers between devices, per_device(): mid_whole = lax.all_gather(mid_stream, 'tp', axis=1, tiled=True)  21.1 us
  transfers between devices with their start and end apart: 9, of which 9 were waited for; matrix products, arithmetic and copies ran while one was open for 3% of the time, Pallas kernels for 0%

commit v1 on v0

--- a/solution.py
+++ b/solution.py
@@ -66,10 +66,17 @@
     mid_whole = lax.all_gather(mid_stream, "tp", axis=1, tiled=True)
     normed_two = rms_scale(mid_whole.astype(jnp.float32), second_gain).astype(jnp.bfloat16)
     column_part = normed_two
+    choose_the_pipes = lambda z, bus_axis: jnp.concatenate(
+        lax.all_to_all(
+            jnp.stack([z for _ in range(lax.axis_size(bus_axis))]),
+            bus_axis,
+            split_axis=0,
+            concat_axis=0,
+        ),
+        axis=0,
+    )
     pre_act = jnp.dot(
-        column_part,
-        lax.all_gather(up_proj, "fs", axis=0, tiled=True),
-        preferred_element_type=jnp.float32,
+        column_part, choose_the_pipes(up_proj, "fs"), preferred_element_type=jnp.float32
     )
     hidden_act = jnp.square(jax.nn.relu(pre_act)).astype(jnp.bfloat16)
     down_terms = jnp.dot(

time: 521 us -> 527 us (1.012)
  starting transfers between devices: 0.31 us -> 6.35 us
    all_to_all x0 -> x1, waiting for transfers between devices: none -> 304 us  [per_device(): lax.all_to_all(jnp.stack([z for _ in range(lax.axis_size(bus_axis))]), bu...]
    all_gather x1, waiting for transfers between devices: 149 us -> 0.01 us  [per_device(): lax.all_gather(down_proj, 'fs', axis=1, tiled=True)]
    all_gather x1 -> x0, waiting for transfers between devices: 149 us -> none  [per_device(): lax.all_gather(up_proj, 'fs', axis=0, tiled=True)]
    all_gather x1, waiting for transfers between devices: 21.1 us -> 11.5 us  [per_device(): mid_whole = lax.all_gather(mid_stream, 'tp', axis=1, tiled=True)]
    all_to_all x0 -> x1, starting transfers between devices: none -> 5.9 us  [per_device(): lax.all_to_all(jnp.stack([z for _ in range(lax.axis_size(bus_axis))]), bu...]
  transfers between devices with their start and end apart: 9 -> 9, of which waited for: 9 -> 8; matrix products, arithmetic and copies ran while one was open for 3% -> 4% of each run, Pallas kernels for 0% -> 0%
where the time goes in v1:
time: 527 us; the launch traced here: 526 us
  waiting for transfers between devices  464 us (88%)
  matrix products  26.3 us (5%)
  between operations  13.6 us (3%)
  other arithmetic  8.82 us (2%)
  local copies, waits for them, and re-layouts  7.23 us (1%)
  starting transfers between devices  6.35 us (1%)
    all_to_all x1, waiting for transfers between devices, per_device(): lax.all_to_all(jnp.stack([z for _ in range(lax.axis_size(bus_axis))]), bu...  304 us
    reduce_scatter x1, waiting for transfers between devices, per_device(): lax.psum_scatter(down_terms.astype(jnp.bfloat16), 'tp', scatter_dimension...  29.7 us
    all_gather x1, waiting for transfers between devices, per_device(): lax.all_gather(v_proj, 'fs', axis=0, tiled=True)  27.5 us
    all_gather x1, waiting for transfers between devices, per_device(): lax.all_gather(mix_proj, 'fs', axis=0, tiled=True)  25.8 us
    all_gather x1, waiting for transfers between devices, per_device(): whole_rows = lax.all_gather(tokens, 'tp', axis=1, tiled=True)  22.8 us
    all_gather x1, waiting for transfers between devices, per_device(): lax.all_gather(u_proj, 'fs', axis=0, tiled=True)  21.6 us
    all_gather x1, waiting for transfers between devices, per_device(): gated_whole = lax.all_gather(gated_vals, 'tp', axis=1, tiled=True)  17.6 us
    dot_general x1, matrix products, per_device(): jnp.dot(hidden_act, lax.all_gather(down_proj, 'fs', axis=1, tiled=True),...  16.6 us
  transfers between devices with their start and end apart: 9, of which 8 were waited for; matrix products, arithmetic and copies ran while one was open for 4% of the time, Pallas kernels for 0%

profile of v1, /device:TPU:0, one launch (start us, length us, event | category | flops | bytes accessed | tf_op | source)
XLA Modules:
  0.0 526.3 jit_solution(17791289159973319721)
XLA Ops:
  6.5 0.7 all-gather.8.cloned.1.call-update
  7.3 0.7 all-gather.12.cloned.1.call-update
  8.1 0.7 all-gather.10.cloned.1.call-update
  9.4 0.7 convert_element_type.58
  11.4 22.8 %all-gather.8.cloned.1.call-done = bf16[512,2048]{1,0:T(8,128)(2,1)} async-done(((bf16[512,512]{1,0:T(8,128)(2,1)}), bf16[512,2048]{1,0:T(8,128)(2,1)}) %all-gather.8.cloned.1.call-update) | async-done | bytes 2097168 | tf_op jit(solution)/shard_map/all_gather | solution.py:27
  34.2 2.1 fusion
  36.3 27.5 %all-gather.12.cloned.1.call-done = bf16[2048,256]{1,0:T(8,128)(2,1)} async-done(((bf16[512,256]{1,0:T(8,128)(2,1)}), bf16[2048,256]{1,0:T(8,128)(2,1)}) %all-gather.12.cloned.1.call-update) | async-done | bytes 1048592 | tf_op jit(solution)/shard_map/all_gather | solution.py:39
  63.8 3.5 fusion.52
  68.3 1.3 reshape.57
  70.2 1.0 copy.26
  71.2 21.6 %all-gather.10.cloned.1.call-done = bf16[2048,256]{1,0:T(8,128)(2,1)} async-done(((bf16[512,256]{1,0:T(8,128)(2,1)}), bf16[2048,256]{1,0:T(8,128)(2,1)}) %all-gather.10.cloned.1.call-update) | async-done | bytes 1048592 | tf_op jit(solution)/shard_map/all_gather | solution.py:34
  92.8 2.9 fusion.33
  95.7 25.8 %all-gather.16.cloned.1.call-done = bf16[1024,512]{1,0:T(8,128)(2,1)} async-done(((bf16[256,512]{1,0:T(8,128)(2,1)}), bf16[1024,512]{1,0:T(8,128)(2,1)}) %all-gather.16.cloned.1.call-update) | async-done | bytes 1048592 | tf_op jit(solution)/shard_map/all_gather | solution.py:62
  121.6 17.6 %all-gather.14.cloned.1.call-done = bf16[512,1024]{1,0:T(8,128)(2,1)} async-done(((bf16[512,256]{1,0:T(8,128)(2,1)}), bf16[512,1024]{1,0:T(8,128)(2,1)}) %all-gather.14.cloned.1.call-update) | async-done | bytes 1048592 | tf_op jit(solution)/shard_map/all_gather | solution.py:58
  139.2 3.0 fusion.9
  142.3 4.3 stack.2
  146.6 5.9 %all-to-all-start = ((bf16[4,512,2048]{2,1,0:T(8,128)(2,1)}), bf16[4,512,2048]{2,1,0:T(8,128)(2,1)}, u32[]{:S(2)}, u32[]{:S(2)}) async-start(bf16[4,512,2048]{2,1,0:T(8,128)(2,1)} %stack.2), calls=%async_computation | async-start | bytes 16777216 | tf_op jit(solution)/shard_map/all_to_all | solution.py:70
  152.6 0.7 all-gather.20.cloned.1.call-update
  153.5 11.5 %all-gather.18.cloned.1.call-done = bf16[512,2048]{1,0:T(8,128)(2,1)} async-done(((bf16[512,512]{1,0:T(8,128)(2,1)}), bf16[512,2048]{1,0:T(8,128)(2,1)}) %all-gather.18.cloned.1.call-update) | async-done | bytes 2097168 | tf_op jit(solution)/shard_map/all_gather | solution.py:66
  165.0 2.1 fusion.3
  167.1 304.0 %all-to-all-done = bf16[4,512,2048]{2,1,0:T(8,128)(2,1)} async-done(((bf16[4,512,2048]{2,1,0:T(8,128)(2,1)}), bf16[4,512,2048]{2,1,0:T(8,128)(2,1)}, u32[]{:S(2)}, u32[]{:S(2)}) %all-to-all-start) | async-done | bytes 8388640 | tf_op jit(solution)/shard_map/all_to_all | solution.py:70
  471.1 16.6 %convolution_convert_fusion = bf16[512,2048]{1,0:T(8,128)(2,1)} fusion(bf16[2048,2048]{1,0:T(8,128)(2,1)} %all-gather.20.cloned.1.call-done, bf16[2048,2048]{1,0:T(8,128)(2,1)} %bitcast.5, bf16[512,2048]{1,0:T(8,128)(2,1)} %all-gather.18.cloned.1.call-done, f32[2048]{0:T(1024)S(1)} %convert_element_type.68, f32[512]{0:T(512)S(1)} %add_rsqrt_fusion.1), kind=kOutput, calls=%fused_computation.11 | convolution fusion | flops 8598323200 | bytes 20981760 | tf_op jit(solution)/shard_map/dot_general | solution.py:82
  487.8 29.7 %reduce-scatter.2.cloned.1.call-done = bf16[512,512]{1,0:T(8,128)(2,1)} async-done(((bf16[512,2048]{1,0:T(8,128)(2,1)}), bf16[512,512]{1,0:T(8,128)(2,1)}) %reduce-scatter.2.cloned.1.call-update) | async-done | bytes 524304 | tf_op jit(solution)/shard_map/reduce_scatter | solution.py:87
  517.4 2.0 add_convert_fusion
  (37 shorter events, 3.9 us)
Async XLA Ops:
  6.5 27.7 %all-gather.8.cloned.1.call-start = ((), (), s32[]{:S(2)}) async-start(), calls=%async_computation.2 | async-start | bytes 2621440 | tf_op jit(solution)/shard_map/all_gather | solution.py:27
  7.3 56.5 %all-gather.12.cloned.1.call-start = ((), (), s32[]{:S(2)}) async-start(), calls=%async_computation.4 | async-start | bytes 1310720 | tf_op jit(solution)/shard_map/all_gather | solution.py:39
  8.0 84.8 %all-gather.10.cloned.1.call-start = ((), (), s32[]{:S(2)}) async-start(), calls=%async_computation.3 | async-start | bytes 1310720 | tf_op jit(solution)/shard_map/all_gather | solution.py:34
  8.7 112.8 %all-gather.16.cloned.1.call-start = ((), (), s32[]{:S(2)}) async-start(), calls=%async_computation.6 | async-start | bytes 1310720 | tf_op jit(solution)/shard_map/all_gather | solution.py:62
  9.3 129.9 %all-gather.14.cloned.1.call-start = ((), (), s32[]{:S(2)}) async-start(), calls=%async_computation.5 | async-start | bytes 1310720 | tf_op jit(solution)/shard_map/all_gather | solution.py:58
  36.3 33.6 %copy-start.4 = (bf16[2,128,128]{2,1,0:T(8,128)(2,1)S(1)}, bf16[2,128,128]{2,1,0:T(8,128)(2,1)}, u32[]{:S(2)}) copy-start(bf16[2,128,128]{2,1,0:T(8,128)(2,1)} %param.16) | copy-start | bytes 196612
  67.3 25.5 %copy-start.2 = (bf16[512,2048]{1,0:T(8,128)(2,1)S(1)}, bf16[512,2048]{1,0:T(8,128)(2,1)}, u32[]{:S(2)}) copy-start(bf16[512,2048]{1,0:T(8,128)(2,1)} %all-gather.8.cloned.1.call-done) | copy-start | bytes 6291460
  70.2 69.1 %copy-start.3 = (bf16[512,512]{1,0:T(8,128)(2,1)S(1)}, bf16[512,512]{1,0:T(8,128)(2,1)}, u32[]{:S(2)}) copy-start(bf16[512,512]{1,0:T(8,128)(2,1)} %param.11) | copy-start | bytes 1572868
  95.7 46.6 %copy-start = (bf16[512,2048]{1,0:T(8,128)(2,1)S(1)}, bf16[512,2048]{1,0:T(8,128)(2,1)}, u32[]{:S(2)}) copy-start(bf16[512,2048]{1,0:T(8,128)(2,1)} %param.20) | copy-start | bytes 6291460
  95.7 69.3 %all-gather.18.cloned.1.call-start = ((), (), s32[]{:S(2)}) async-start(), calls=%async_computation.7 | async-start | bytes 2621440 | tf_op jit(solution)/shard_map/all_gather | solution.py:66
  146.6 6.9 %copy-start.5 = (bf16[2048]{0:T(1024)(128)(2,1)S(1)}, bf16[2048]{0:T(1024)(128)(2,1)}, u32[]{:S(2)}) copy-start(bf16[2048]{0:T(1024)(128)(2,1)} %param.19) | copy-start | bytes 12292
  146.6 324.5 %all-to-all-start = ((bf16[4,512,2048]{2,1,0:T(8,128)(2,1)}), bf16[4,512,2048]{2,1,0:T(8,128)(2,1)}, u32[]{:S(2)}, u32[]{:S(2)}) async-start(bf16[4,512,2048]{2,1,0:T(8,128)(2,1)} %stack.2), calls=%async_computation | async-start | bytes 16777216 | tf_op jit(solution)/shard_map/all_to_all | solution.py:70
  152.5 318.6 %all-gather.20.cloned.1.call-start = ((), (), s32[]{:S(2)}) async-start(), calls=%async_computation.8 | async-start | bytes 10485760 | tf_op jit(solution)/shard_map/all_gather | solution.py:84
  153.3 364.2 %reduce-scatter.2.cloned.1.call-start = ((), (), s32[]{:S(2)}) async-start(), calls=%async_computation.9 | async-start | bytes 2621440 | tf_op jit(solution)/shard_map/reduce_scatter | solution.py:87
  471.1 46.3 %copy-start.1 = (bf16[512,512]{1,0:T(8,128)(2,1)S(1)}, bf16[512,512]{1,0:T(8,128)(2,1)}, u32[]{:S(2)}) copy-start(bf16[512,512]{1,0:T(8,128)(2,1)} %fusion.9) | copy-start | bytes 1572868
Sparse Core Ops, SparseCore 0:
  8.9 25.2 all-gather.7
  35.8 27.9 all-gather.11
  65.4 27.3 all-gather.9
  94.2 27.3 all-gather.15
  123.0 16.1 all-gather.13
  142.4 22.5 all-gather.17
  166.6 283.2 all-gather.19
  487.9 29.5 reduce-scatter.1
